TPU v7x, 32 devices: a whole 2x2x4 slice. The times are simulated.
32 devices in a mesh: sp: 8 (over z, x), tp: 4 (over y, core).
Axes of the slice: x: 2, y: 2, z: 4, core: 2. Of those that a mesh axis runs over, the one named last changes fastest.
Arguments:
- latent: bfloat16 [9216, 2048], P(('sp', 'tp')), may hold values from -0.6 to 0.6
- context: bfloat16 [32, 2048], P(('sp', 'tp')), may hold values from -6 to 6
- condition: float32 [2048], P('sp'), may hold values from -6 to 6
- context_condition: float32 [2048], P('sp'), may hold values from -6 to 6
- modulation_weight: bfloat16 [2048, 6144], P('sp', 'tp'), may hold values from -0.1875 to 0.1875
- norm_gain: float32 [2048], replicated, may hold values from 0.1 to 1.9
- query_weight: bfloat16 [2048, 1024], replicated
- key_weight: bfloat16 [2048, 256], replicated
- value_weight: bfloat16 [2048, 256], replicated, may hold values from -0.125 to 0.125
- output_weight: bfloat16 [1024, 2048], replicated, may hold values from -0.1875 to 0.1875
- query_gain: float32 [128], replicated, may hold values from 0.5 to 6
- key_gain: float32 [128], replicated, may hold values from 0.5 to 6
- sink_logit: float32 [8], replicated, may hold values from 1 to 5
Outputs:
- updated: bfloat16 [9216, 2048], P(('sp', 'tp'))
All inputs are finite; a program needn't handle non-finite values.
Results may differ from a plain program's by a relative error of at most 0.006.
The roundings to bfloat16 on the way count: a program that leaves them out, or rounds other values in their place, can miss the bound.
Values may be sent and summed in bfloat16 or wider, within the bound.
A program may use at most 64 MiB of HBM per device.

v0:
```python
import jax
import jax.numpy as jnp
from jax import lax
from jax.sharding import PartitionSpec as P

WINDOW = 128
GRID_W = 64
EPS = 1e-06
ROPE_BASE = 10000.0
FAR_LOGIT = -1e30


def with_halo(array, sides, width):
    for axis, dim in sides:
        size, length = (lax.axis_size(axis), array.shape[dim])
        up = [(i, (i + 1) % size) for i in range(size - 1)]
        down = [(j, i) for i, j in up]
        last = lax.slice_in_dim(array, length - width, length, axis=dim)
        first = lax.slice_in_dim(array, 0, width, axis=dim)
        before = lax.ppermute(last, axis, up)
        after = lax.ppermute(first, axis, down)
        array = jnp.concatenate([before, array, after], axis=dim)
    return array


def rms_rows(values_in):
    return values_in * lax.rsqrt(jnp.mean(values_in * values_in, axis=-1, keepdims=True) + EPS)


def turn_halves(halves_in):
    former, latter = jnp.split(halves_in, 2, axis=-1)
    return jnp.concatenate([-latter, former], axis=-1)


def rotary(values_in, positions):
    quarter = values_in.shape[-1] // 4
    inverse = jnp.power(ROPE_BASE, -jnp.arange(quarter, dtype=jnp.float32) / quarter)
    by_rows = (positions // GRID_W).astype(jnp.float32)[:, None] * inverse
    by_cols = (positions % GRID_W).astype(jnp.float32)[:, None] * inverse
    angles = jnp.concatenate([by_rows, by_rows, by_cols, by_cols], axis=-1)[:, None, :]
    row_half, col_half = jnp.split(values_in, 2, axis=-1)
    turned = jnp.concatenate([turn_halves(row_half), turn_halves(col_half)], axis=-1)
    return values_in * jnp.cos(angles) + turned * jnp.sin(angles)


def head_norm(flat, gain):
    per_head = flat.reshape(flat.shape[0], flat.shape[1] // gain.shape[0], gain.shape[0])
    return rms_rows(per_head) * gain


def modulated(tokens_in, norm_gain, shift, scale):
    values_in = tokens_in.astype(jnp.float32)
    return (rms_rows(values_in) * norm_gain * (1.0 + scale) + shift).astype(jnp.bfloat16)


def key_value_rows(hidden_rows, positions, key_weight, value_weight, key_gain):
    row_count = hidden_rows.shape[0]
    kv_width = key_weight.shape[1]
    keys = (
        rotary(
            head_norm(
                jnp.dot(hidden_rows, key_weight, preferred_element_type=jnp.float32), key_gain
            ),
            positions,
        )
        .astype(jnp.bfloat16)
        .reshape(row_count, kv_width)
    )
    values = jnp.dot(hidden_rows, value_weight, preferred_element_type=jnp.float32).astype(
        jnp.bfloat16
    )
    return jnp.stack([keys, values])


def attend(queries, keys, values, ctx_keys, ctx_values, sink_logit, allowed, head_size):
    row_count = queries.shape[0]
    kv_count = keys.shape[1] // head_size
    group = queries.shape[1] // keys.shape[1]
    score_scale = head_size ** (-0.5)
    grouped = queries.reshape(row_count, kv_count, group, head_size)
    near_keys = keys.reshape(keys.shape[0], kv_count, head_size)
    near_values = values.reshape(values.shape[0], kv_count, head_size)
    far_keys = ctx_keys.reshape(ctx_keys.shape[0], kv_count, head_size)
    far_values = ctx_values.reshape(ctx_values.shape[0], kv_count, head_size)
    near_scores = (
        jnp.einsum("rhgd,khd->hgrk", grouped, near_keys, preferred_element_type=jnp.float32)
        * score_scale
    )
    near_scores = jnp.where(allowed, near_scores, FAR_LOGIT)
    ctx_scores = (
        jnp.einsum("rhgd,khd->hgrk", grouped, far_keys, preferred_element_type=jnp.float32)
        * score_scale
    )
    sink_part = sink_logit.reshape(kv_count, group)[:, :, None, None]
    row_max = jnp.maximum(
        jnp.maximum(
            jnp.max(near_scores, axis=-1, keepdims=True),
            jnp.max(ctx_scores, axis=-1, keepdims=True),
        ),
        sink_part,
    )
    near_exp = jnp.exp(near_scores - row_max)
    ctx_exp = jnp.exp(ctx_scores - row_max)
    denominator = (
        jnp.sum(near_exp, axis=-1, keepdims=True)
        + jnp.sum(ctx_exp, axis=-1, keepdims=True)
        + jnp.exp(sink_part - row_max)
    )
    near_probs = (near_exp / denominator).astype(jnp.bfloat16)
    ctx_probs = (ctx_exp / denominator).astype(jnp.bfloat16)
    mixed = jnp.einsum(
        "hgrk,khd->rhgd", near_probs, near_values, preferred_element_type=jnp.float32
    ) + jnp.einsum("hgrk,khd->rhgd", ctx_probs, far_values, preferred_element_type=jnp.float32)
    return mixed.astype(jnp.bfloat16).reshape(row_count, queries.shape[1])


def local(
    latent,
    context,
    condition,
    context_condition,
    modulation_weight,
    norm_gain,
    query_weight,
    key_weight,
    value_weight,
    output_weight,
    query_gain,
    key_gain,
    sink_logit,
):
    model_width = latent.shape[1]
    head_size = query_gain.shape[0]
    kv_width = key_weight.shape[1]
    query_width = query_weight.shape[1]
    activations = jax.nn.silu(jnp.stack([condition, context_condition])).astype(jnp.bfloat16)
    partial_value = jnp.dot(activations, modulation_weight, preferred_element_type=jnp.float32)
    summed = lax.psum(partial_value, "sp")
    modulation = lax.all_gather(summed, "tp", axis=1, tiled=True)
    hidden = modulated(
        latent, norm_gain, modulation[0, :model_width], modulation[0, model_width : 2 * model_width]
    )
    ctx_hidden = modulated(
        context,
        norm_gain,
        modulation[1, :model_width],
        modulation[1, model_width : 2 * model_width],
    )
    gate = modulation[0, 2 * model_width :]
    row_count = latent.shape[0]
    row_start = lax.axis_index(("sp", "tp")) * row_count
    total_rows = row_count * lax.axis_size(("sp", "tp"))
    positions = row_start + jnp.arange(row_count, dtype=jnp.int32)
    queries = (
        rotary(
            head_norm(
                jnp.dot(hidden, query_weight, preferred_element_type=jnp.float32), query_gain
            ),
            positions,
        )
        .astype(jnp.bfloat16)
        .reshape(row_count, query_width)
    )
    local_both = key_value_rows(hidden, positions, key_weight, value_weight, key_gain)
    band = with_halo(local_both, ((("sp", "tp"), 1),), WINDOW)
    ctx_piece = lax.all_gather(ctx_hidden, ("sp", "tp"), axis=0, tiled=True)
    piece_rows = ctx_piece.shape[0]
    projected = head_norm(
        jnp.dot(ctx_piece, key_weight, preferred_element_type=jnp.float32), key_gain
    )
    projected = projected.astype(jnp.bfloat16).reshape(piece_rows, kv_width)
    value_rows = jnp.dot(ctx_piece, value_weight, preferred_element_type=jnp.float32).astype(
        jnp.bfloat16
    )
    ctx_both = jnp.concatenate([projected, value_rows], axis=1)
    key_pos = row_start - WINDOW + jnp.arange(row_count + 2 * WINDOW, dtype=jnp.int32)
    allowed = (
        (jnp.abs(key_pos[None, :] - positions[:, None]) <= WINDOW)
        & (key_pos[None, :] >= 0)
        & (key_pos[None, :] < total_rows)
    )
    mixed = attend(
        queries,
        band[0],
        band[1],
        ctx_both[:, :kv_width],
        ctx_both[:, kv_width:],
        sink_logit,
        allowed,
        head_size,
    )
    update = jnp.dot(mixed, output_weight, preferred_element_type=jnp.float32)
    return (latent.astype(jnp.float32) + gate * update).astype(jnp.bfloat16)


def solution(mesh):
    placed = (
        P(("sp", "tp"), None),
        P(("sp", "tp"), None),
        P("sp"),
        P("sp"),
        P("sp", "tp"),
        P(),
        P(),
        P(),
        P(),
        P(),
        P(),
        P(),
        P(),
    )
    return jax.shard_map(
        local, mesh=mesh, in_specs=placed, out_specs=P(("sp", "tp"), None), check_vma=False
    )
```

profile of v0, /device:TPU:0, one launch (start us, length us, event | category | flops | bytes accessed | tf_op | source)
XLA Modules:
  0.0 136.5 jit_solution(12055852137158894293)
XLA Ops:
  0.0 1.5 %multiply_reduce_fusion.3 = f32[]{:T(128)} fusion(bf16[1,2048]{1,0:T(2,128)(2,1)} %param.14), kind=kLoop, calls=%fused_computation.85 | loop fusion | flops 6143 | bytes 4100 | tf_op jit(solution)/shard_map/reduce_sum | solution.py:27
  2.2 0.7 broadcast_bitcast_fusion
  2.9 1.6 %fusion.4 = f32[288]{0:T(512)S(1)} fusion(bf16[288,2048]{1,0:T(8,128)(2,1)} %param.13), kind=kLoop, calls=%fused_computation.11 | loop fusion | flops 1769184 | bytes 1180800 | tf_op jit(solution)/shard_map/reduce_sum | solution.py:27
  4.5 1.4 %fusion.49 = f32[2,1536]{1,0:T(2,128)S(1)} fusion(bf16[256,1536]{1,0:T(8,128)(2,1)} %param.17, f32[1,256]{1,0:T(1,128)} %bitcast.97, f32[1,256]{1,0:T(1,128)} %bitcast.98), kind=kOutput, calls=%fused_computation.105 | convolution fusion | flops 1575936 | bytes 800768 | tf_op jit(solution)/shard_map/dot_general | solution.py:137
  5.9 38.9 %psum.7 = f32[2,1536]{1,0:T(2,128)S(1)} all-reduce(f32[2,1536]{1,0:T(2,128)S(1)} %fusion.49), channel_id=1, replica_groups=mesh['sp'=8,'tp'=4] {'sp'}, use_global_device_ids=true, to_apply=%region_0.1 | all-reduce | flops 3072 | bytes 24576 | tf_op jit(solution)/shard_map/psum | solution.py:138
  44.7 5.2 %all_gather.6 = f32[2,6144]{1,0:T(2,128)S(1)} all-gather(f32[2,1536]{1,0:T(2,128)S(1)} %psum.7), channel_id=1, replica_groups=mesh['sp'=8,'tp'=4] {'tp'}, dimensions={1}, use_global_device_ids=true | all-gather | bytes 61440 | tf_op jit(solution)/shard_map/all_gather | solution.py:139
  49.9 0.6 fusion.62
  50.6 0.6 fusion.16
  51.2 0.6 copy-done.9
  51.8 0.6 fusion.59
  52.4 0.2 reshape.279
  52.6 0.4 multiply_reduce_fusion.1
  53.1 0.4 multiply_multiply_fusion.1
  53.5 1.0 slice_negate_fusion.3
  54.6 0.6 fusion.37
  55.3 1.0 maximum_multiply_fusion.1
  56.3 0.4 mul.272
  56.9 0.7 pad_maximum_fusion.3
  57.6 2.9 %collective-permute-start = (bf16[2,128,256]{2,1,0:T(8,128)(2,1)}, bf16[2,128,256]{2,1,0:T(8,128)(2,1)}, u32[]{:S(2)}, u32[]{:S(2)}) collective-permute-start(bf16[2,128,256]{2,1,0:T(8,128)(2,1)} %get-tuple-element.11), channel_id=1, source_target_pairs={{0,1},{1,2},{2,3},{3,4},{4,5},{5,6},{6,7},{7,8},{8,9},{9,10},{10,1... | collective-permute-start | bytes 393224 | tf_op jit(solution)/shard_map/ppermute | solution.py:20
  60.5 1.3 collective-permute-start.1
  61.8 0.6 iota_add_fusion.1
  62.4 0.6 fusion.41
  63.0 40.1 %all-gather = bf16[32,1,2048]{2,1,0:T(2,128)(2,1)S(1)} all-gather(bf16[1,1,2048]{2,1,0:T(2,128)(2,1)S(1)} %get-tuple-element.20), channel_id=1, replica_groups=mesh['sp'=8,'tp'=4] {'sp','tp'}, dimensions={0}, use_global_device_ids=true | all-gather | bytes 135168 | tf_op jit(solution)/shard_map/all_gather | solution.py:166
  103.0 0.3 convolution_convert_fusion.1
  103.3 0.3 fusion.29
  103.6 4.0 %fusion.56 = f32[288,1024]{1,0:T(8,128)S(1)} fusion(bf16[2048,1024]{1,0:T(8,128)(2,1)} %param.19, bf16[288,2048]{1,0:T(8,128)(2,1)} %param.13, f32[2048]{0:T(1024)S(1)} %bitcast.93, f32[2048]{0:T(1024)S(1)} %bitcast.96, f32[2048]{0:T(1024)S(1)} %copy-done.15, f32[288]{0:T(512)S(1)} %add_rsqrt_fusion.3), kind=kOutput, calls=%fused_computation.113 | convolution fusion | flops 1211498496 | bytes 6579328 | tf_op jit(solution)/shard_map/dot_general | solution.py:157
  107.6 1.0 copy-done.2
  108.6 1.6 %reshape.280 = f32[288,2,4,128]{3,2,1,0:T(4,128)} reshape(f32[288,1024]{1,0:T(8,128)S(1)} %fusion.56) | data formatting | bytes 2359296 | tf_op jit(solution)/shard_map/reshape | solution.py:47
  110.2 1.7 %copy.60 = f32[288,1024]{0,1:T(8,128)S(1)} copy(f32[288,1024]{1,0:T(8,128)} %copy-done.2) | data formatting | bytes 2359296 | tf_op jit(solution)/shard_map/dot_general | solution.py:157
  112.0 0.7 max.30
  112.9 0.1 multiply_reduce_fusion
  113.1 0.3 multiply_multiply_fusion
  113.5 1.4 %copy.65 = f32[288,2,4,32]{3,0,2,1:T(8,128)} copy(f32[288,2,4,32]{0,3,2,1:T(8,128)S(1)} %bitcast.82) | data formatting | bytes 589824 | tf_op jit(solution)/shard_map/concatenate | solution.py:42
  114.9 1.4 %copy.62 = f32[288,2,4,32]{3,0,2,1:T(8,128)} copy(f32[288,2,4,32]{0,3,2,1:T(8,128)S(1)} %bitcast.81) | data formatting | bytes 589824 | tf_op jit(solution)/shard_map/concatenate | solution.py:42
  116.3 1.4 %copy.64 = f32[288,2,4,32]{3,0,2,1:T(8,128)} copy(f32[288,2,4,32]{0,3,2,1:T(8,128)S(1)} %bitcast.80) | data formatting | bytes 589824 | tf_op jit(solution)/shard_map/concatenate | solution.py:42
  117.7 1.4 %copy.63 = f32[288,2,4,32]{3,0,2,1:T(8,128)} copy(f32[288,2,4,32]{0,3,2,1:T(8,128)S(1)} %bitcast.79) | data formatting | bytes 589824 | tf_op jit(solution)/shard_map/concatenate | solution.py:42
  119.2 3.7 %fusion.13 = bf16[288,2,4,128]{3,0,2,1:T(8,128)(2,1)S(1)} fusion(f32[288,2,4,32]{3,0,2,1:T(8,128)} %copy.65, f32[288,2,4,32]{3,0,2,1:T(8,128)} %copy.64, f32[288,2,4,32]{3,0,2,1:T(8,128)} %copy.63, f32[288,2,4,32]{3,0,2,1:T(8,128)} %copy.62, f32[288,2,4,128]{3,2,1,0:T(4,128)S(1)} %copy-done.1, f32[288,128]{1,0:T(8,128)S(1)} %get-tuple-element.18, ...), kind=kLoop, calls=%fused_computation.25 | loop fusion | flops 2654208 | bytes 3253760 | tf_op jit(solution)/shard_map/convert_element_type | solution.py:161
  122.8 0.4 fusion.63
  123.2 0.3 fusion.18
  123.6 1.0 pad_maximum_fusion
  124.8 1.5 %fusion.1 = (f32[2,4,288]{2,1,0:T(4,128)S(1)}, f32[2,544,288,4]{1,2,3,0:T(8,128)S(1)}) fusion(pred[288,544]{1,0:T(8,128)(4,1)S(1)} %fusion.18, bf16[288,2,4,128]{3,0,2,1:T(8,128)(2,1)S(1)} %fusion.13, bf16[544,2,128,1]{2,1,0,3:T(2,128)(2,1)S(1)} %bitcast.86), kind=kOutput, calls=%fused_computation.4 | convolution fusion | flops 324622080 | bytes 6047744 | tf_op jit(solution)/shard_map/rhgd,khd->hgrk/dot_general | solution.py:86
  126.4 2.0 %fusion = f32[2,4,288]{2,1,0:T(4,128)S(1)} fusion(f32[2,544,288,4]{1,2,3,0:T(8,128)S(1)} %get-tuple-element.26, f32[2,4,288]{2,1,0:T(4,128)S(1)} %maximum_maximum_fusion, pred[288,544]{1,0:T(8,128)(4,1)S(1)} %fusion.18), kind=kLoop, calls=%fused_computation.3 | loop fusion | flops 5011200 | bytes 5188608 | tf_op jit(solution)/shard_map/reduce_sum | solution.py:105
  128.5 1.7 %fusion.2 = f32[2,128,4,288]{1,3,2,0:T(8,128)S(1)} fusion(f32[2,544,288,4]{1,2,3,0:T(8,128)S(1)} %get-tuple-element.26, f32[2,4,288]{2,1,0:T(4,128)S(1)} %exponential_add_fusion, f32[2,4,288]{2,1,0:T(4,128)S(1)} %maximum_maximum_fusion, pred[288,544]{1,0:T(8,128)(4,1)S(1)} %fusion.18, bf16[544,2,128,1]{2,1,0,3:T(2,128)(2,1)S(1)} %bitcast.87), kind=kOutput, calls=%fused_computation.8 | convolution fusion | flops 327131136 | bytes 6646784 | tf_op jit(solution)/shard_map/hgrk,khd->rhgd/dot_general | solution.py:111
  130.2 0.4 fusion.10
  130.6 0.3 copy.70
  130.9 0.4 reshape.284
  131.4 0.5 copy-done.6
  131.9 4.6 %fusion.3 = bf16[288,2048]{1,0:T(8,128)(2,1)} fusion(bf16[288,1024]{1,0:T(8,128)(2,1)S(1)} %reshape.284, bf16[1024,2048]{1,0:T(8,128)(2,1)} %param.22, bf16[288,2048]{1,0:T(8,128)(2,1)S(1)} %copy-done.6, f32[2048]{0:T(1024)S(1)} %bitcast.90), kind=kOutput, calls=%fused_computation.10 | convolution fusion | flops 1210318848 | bytes 7151616 | tf_op jit(solution)/shard_map/dot_general | solution.py:192
  (69 shorter events, 1.4 us)
Async XLA Ops:
  0.0 50.5 %copy-start = (bf16[2048,256]{1,0:T(8,128)(2,1)S(1)}, bf16[2048,256]{1,0:T(8,128)(2,1)}, u32[]{:S(2)}) copy-start(bf16[2048,256]{1,0:T(8,128)(2,1)} %param.21) | copy-start | bytes 3145732
  0.0 49.9 %copy-start.13 = (bf16[1,2048]{1,0:T(2,128)(2,1)S(1)}, bf16[1,2048]{1,0:T(2,128)(2,1)}, u32[]{:S(2)}) copy-start(bf16[1,2048]{1,0:T(2,128)(2,1)} %param.14) | copy-start | bytes 12292
  0.0 50.5 %copy-start.5 = (bf16[288,2048]{1,0:T(8,128)(2,1)S(1)}, bf16[288,2048]{1,0:T(8,128)(2,1)}, u32[]{:S(2)}) copy-start(bf16[288,2048]{1,0:T(8,128)(2,1)} %param.13) | copy-start | bytes 3538948
  0.0 49.9 %copy-start.15 = (f32[2048]{0:T(1024)S(1)}, f32[2048]{0:T(1024)}, u32[]{:S(2)}) copy-start(f32[2048]{0:T(1024)} %param.18) | copy-start | bytes 24580
  50.5 1.2 copy-start.9
  51.8 5.1 %copy-start.11 = (bf16[1,288,256]{2,1,0:T(8,128)(2,1)}, bf16[1,288,256]{2,1,0:T(8,128)(2,1)S(1)}, u32[]{:S(2)}) copy-start(bf16[1,288,256]{2,1,0:T(8,128)(2,1)S(1)} %fusion.16) | copy-start | bytes 442372
  51.8 1.4 copy-start.20
  52.4 0.7 copy-start.7
  54.6 2.1 %copy-start.8 = (f32[288,256]{1,0:T(8,128)S(1)}, f32[288,256]{1,0:T(8,128)}, u32[]{:S(2)}) copy-start(f32[288,256]{1,0:T(8,128)} %copy-done.7) | copy-start | bytes 884740
  55.3 1.6 %copy-start.3 = (f32[288,128]{1,0:T(8,128)}, f32[288,128]{1,0:T(8,128)S(1)}, u32[]{:S(2)}) copy-start(f32[288,128]{1,0:T(8,128)S(1)} %get-tuple-element.17) | copy-start | bytes 442372
  56.9 46.5 %copy-start.10 = (bf16[2048,256]{1,0:T(8,128)(2,1)S(1)}, bf16[2048,256]{1,0:T(8,128)(2,1)}, u32[]{:S(2)}) copy-start(bf16[2048,256]{1,0:T(8,128)(2,1)} %param.20) | copy-start | bytes 3145732
  57.6 66.0 %collective-permute-start = (bf16[2,128,256]{2,1,0:T(8,128)(2,1)}, bf16[2,128,256]{2,1,0:T(8,128)(2,1)}, u32[]{:S(2)}, u32[]{:S(2)}) collective-permute-start(bf16[2,128,256]{2,1,0:T(8,128)(2,1)} %get-tuple-element.11), channel_id=1, source_target_pairs={{0,1},{1,2},{2,3},{3,4},{4,5},{5,6},{6,7},{7,8},{8,9},{9,10},{10,1... | collective-permute-start | bytes 393224 | tf_op jit(solution)/shard_map/ppermute | solution.py:20
  60.5 63.1 %collective-permute-start.1 = (bf16[2,128,256]{2,1,0:T(8,128)(2,1)}, bf16[2,128,256]{2,1,0:T(8,128)(2,1)}, u32[]{:S(2)}, u32[]{:S(2)}) collective-permute-start(bf16[2,128,256]{2,1,0:T(8,128)(2,1)} %get-tuple-element.12), channel_id=1, source_target_pairs={{1,0},{2,1},{3,2},{4,3},{5,4},{6,5},{7,6},{8,7},{9,8},{10,9},{11,1... | collective-permute-start | bytes 393224 | tf_op jit(solution)/shard_map/ppermute | solution.py:21
  107.6 1.0 copy-start.2
  110.2 1.8 %copy-start.23 = (f32[8]{0:T(128)S(1)}, f32[8]{0:T(128)}, u32[]{:S(2)}) copy-start(f32[8]{0:T(128)} %param.25) | copy-start | bytes 100
  111.9 1.1 copy-start.21
  116.3 2.8 %copy-start.1 = (f32[288,2,4,128]{3,2,1,0:T(4,128)S(1)}, f32[288,2,4,128]{3,2,1,0:T(4,128)}, u32[]{:S(2)}) copy-start(f32[288,2,4,128]{3,2,1,0:T(4,128)} %reshape.280) | copy-start | bytes 3538948
  117.7 1.4 %copy-start.4 = (f32[288,128]{1,0:T(8,128)S(1)}, f32[288,128]{1,0:T(8,128)}, u32[]{:S(2)}) copy-start(f32[288,128]{1,0:T(8,128)} %copy-done.3) | copy-start | bytes 442372
  117.7 1.4 %copy-start.22 = (f32[128]{0:T(128)S(1)}, f32[128]{0:T(128)}, u32[]{:S(2)}) copy-start(f32[128]{0:T(128)} %param.23) | copy-start | bytes 1540
  119.1 4.1 %copy-start.14 = (s32[288]{0:T(512)S(1)}, s32[288]{0:T(512)}, u32[]{:S(2)}) copy-start(s32[288]{0:T(512)} %iota_add_fusion.1) | copy-start | bytes 3460
  119.1 4.1 %copy-start.17 = (pred[544]{0:T(1024)(128)(4,1)S(1)}, pred[544]{0:T(1024)(128)(4,1)}, u32[]{:S(2)}) copy-start(pred[544]{0:T(1024)(128)(4,1)} %get-tuple-element.31) | copy-start | bytes 1636
  119.2 4.1 %copy-start.18 = (pred[544]{0:T(1024)(128)(4,1)S(1)}, pred[544]{0:T(1024)(128)(4,1)}, u32[]{:S(2)}) copy-start(pred[544]{0:T(1024)(128)(4,1)} %get-tuple-element.32) | copy-start | bytes 1636
  119.2 4.4 %copy-start.12 = (bf16[1,288,256]{2,1,0:T(8,128)(2,1)S(1)}, bf16[1,288,256]{2,1,0:T(8,128)(2,1)}, u32[]{:S(2)}) copy-start(bf16[1,288,256]{2,1,0:T(8,128)(2,1)} %copy-done.11) | copy-start | bytes 442372
  124.8 1.5 %copy-start.19 = (f32[2,4]{1,0:T(2,128)S(1)}, f32[2,4]{1,0:T(2,128)}, u32[]{:S(2)}) copy-start(f32[2,4]{1,0:T(2,128)} %max.30) | copy-start | bytes 100
  130.6 1.3 copy-start.6
  130.6 1.3 copy-start.16
where the time goes:
time: 137 us
  blocking collectives  84.1 us (61%)
  other arithmetic  17.2 us (13%)
  matrix products  15.7 us (11%)
  local copies, waits for them, and re-layouts  14.1 us (10%)
  starting transfers between devices  4.17 us (3%)
    all_gather x1, blocking collectives, local(): ctx_piece = lax.all_gather(ctx_hidden, ('sp', 'tp'), axis=0, tiled=True)  40.1 us
    psum x1, blocking collectives, local(): summed = lax.psum(partial_value, 'sp')  38.9 us
    concatenate x4, local copies, waits for them, and re-layouts, rotary(): jnp.concatenate([turn_halves(row_half), turn_halves(col_half)], axis=-1)  5.6 us
    all_gather x1, blocking collectives, local(): modulation = lax.all_gather(summed, 'tp', axis=1, tiled=True)  5.2 us
    dot_general x1, matrix products, local(): update = jnp.dot(mixed, output_weight, preferred_element_type=jnp.float32)  4.63 us
    dot_general x1, matrix products, local(): jnp.dot(hidden, query_weight, preferred_element_type=jnp.float32)  3.99 us
    reduce_sum x5, other arithmetic, rms_rows(): jnp.mean(values_in * values_in, axis=-1, keepdims=True) + EPS  3.68 us
    convert_element_type x1, other arithmetic, local(): queries = rotary(head_norm(jnp.dot(hidden, query_weight, preferred_elemen...  3.66 us
  transfers between devices with their start and end apart: 2, of which 0 were waited for; matrix products, arithmetic and copies ran while one was open for 15% of the time, Pallas kernels for 0%

commit v1 on v0

--- a/solution.py
+++ b/solution.py
@@ -163,7 +163,10 @@
     )
     local_both = key_value_rows(hidden, positions, key_weight, value_weight, key_gain)
     band = with_halo(local_both, ((("sp", "tp"), 1),), WINDOW)
-    ctx_piece = lax.all_gather(ctx_hidden, ("sp", "tp"), axis=0, tiled=True)
+    ctx_piece = jnp.concatenate(
+        lax.all_to_all(jnp.stack([ctx_hidden] * lax.axis_size(("sp", "tp"))), ("sp", "tp"), 0, 0),
+        axis=0,
+    )
     piece_rows = ctx_piece.shape[0]
     projected = head_norm(
         jnp.dot(ctx_piece, key_weight, preferred_element_type=jnp.float32), key_gain

time: 137 us -> 110 us (0.80)
  the two profiles are of different devices: /device:TPU:0 before, /device:TPU:8 now
where the time goes in v1:
time: 110 us
  blocking collectives  39.8 us (36%)
  other arithmetic  18.7 us (17%)
  local copies, waits for them, and re-layouts  18.4 us (17%)
  matrix products  18.4 us (17%)
  starting transfers between devices  13.5 us (12%)
  between operations  1.23 us (1%)
    psum x1, blocking collectives, local(): summed = lax.psum(partial_value, 'sp')  34.6 us
    all_to_all x1, starting transfers between devices, local(): lax.all_to_all(jnp.stack([ctx_hidden] * lax.axis_size(('sp', 'tp'))), ('s...  6.13 us
    concatenate x4, local copies, waits for them, and re-layouts, rotary(): jnp.concatenate([turn_halves(row_half), turn_halves(col_half)], axis=-1)  5.62 us
    ppermute x1, starting transfers between devices, with_halo(): after = lax.ppermute(first, axis, down)  5.33 us
    all_gather x1, blocking collectives, local(): modulation = lax.all_gather(summed, 'tp', axis=1, tiled=True)  5.2 us
    unnamed x46, local copies, waits for them, and re-layouts  4.77 us
    dot_general x1, matrix products, local(): update = jnp.dot(mixed, output_weight, preferred_element_type=jnp.float32)  4.63 us
    reduce_sum x1, other arithmetic, attend(): jnp.sum(near_exp, axis=-1, keepdims=True)  4.06 us
  transfers between devices with their start and end apart: 3, of which 0 were waited for; matrix products, arithmetic and copies ran while one was open for 29% of the time, Pallas kernels for 0%

profile of v1, /device:TPU:8, one launch (start us, length us, event | category | flops | bytes accessed | tf_op | source)
XLA Modules:
  0.0 109.9 jit_solution(10305082633566375653)
XLA Ops:
  0.0 1.5 %multiply_reduce_fusion.3 = f32[]{:T(128)} fusion(bf16[1,2048]{1,0:T(2,128)(2,1)} %param.14), kind=kLoop, calls=%fused_computation.84 | loop fusion | flops 6143 | bytes 4100 | tf_op jit(solution)/shard_map/reduce_sum | solution.py:27
  2.2 1.4 %fusion.51 = f32[2,1536]{1,0:T(2,128)S(1)} fusion(bf16[256,1536]{1,0:T(8,128)(2,1)} %param.17, f32[1,256]{1,0:T(1,128)} %bitcast.107, f32[1,256]{1,0:T(1,128)} %bitcast.108), kind=kOutput, calls=%fused_computation.105 | convolution fusion | flops 1575936 | bytes 800768 | tf_op jit(solution)/shard_map/dot_general | solution.py:137
  3.6 34.6 %psum.7 = f32[2,1536]{1,0:T(2,128)S(1)} all-reduce(f32[2,1536]{1,0:T(2,128)S(1)} %fusion.51), channel_id=1, replica_groups=mesh['sp'=8,'tp'=4] {'sp'}, use_global_device_ids=true, to_apply=%region_0.1 | all-reduce | flops 3072 | bytes 24576 | tf_op jit(solution)/shard_map/psum | solution.py:138
  38.1 5.2 %all_gather.3 = f32[2,6144]{1,0:T(2,128)S(1)} all-gather(f32[2,1536]{1,0:T(2,128)S(1)} %psum.7), channel_id=1, replica_groups=mesh['sp'=8,'tp'=4] {'tp'}, dimensions={1}, use_global_device_ids=true | all-gather | bytes 61440 | tf_op jit(solution)/shard_map/all_gather | solution.py:139
  43.3 0.8 fusion.42
  44.2 0.5 broadcast.259
  44.7 1.4 %reduce.3 = bf16[32,2048]{1,0:T(8,128)(2,1)S(1)} reduce(bf16[32,1,2048]{2,1,0:T(2,128)(2,1)S(1)} %stack.17, bf16[]{:T(256)} %broadcast.259), dimensions={1}, to_apply=%stack.17.reduce_sub_computation | reduce | bytes 262146 | tf_op jit(solution)/shard_map/stack | solution.py:167
  46.1 0.7 reshape.297
  46.9 6.1 %all-to-all-start = ((bf16[32,2,1024]{2,1,0:T(2,128)(2,1)}), bf16[32,2,1024]{2,1,0:T(2,128)(2,1)}, u32[]{:S(2)}, u32[]{:S(2)}) async-start(bf16[32,2,1024]{2,1,0:T(2,128)(2,1)} %reshape.297), calls=%async_computation | async-start | bytes 262144 | tf_op jit(solution)/shard_map/all_to_all | solution.py:167
  53.1 0.3 fusion.4
  53.5 0.6 fusion.16
  54.1 0.6 copy-done.11
  54.7 0.6 fusion.61
  55.5 0.4 multiply_reduce_fusion.1
  56.0 0.4 multiply_multiply_fusion.1
  56.4 1.0 slice_negate_fusion.3
  57.5 0.6 fusion.39
  58.2 1.0 maximum_multiply_fusion.1
  59.2 0.4 mul.272
  59.8 0.7 pad_maximum_fusion.3
  60.5 2.0 %collective-permute-start = (bf16[2,128,256]{2,1,0:T(8,128)(2,1)}, bf16[2,128,256]{2,1,0:T(8,128)(2,1)}, u32[]{:S(2)}, u32[]{:S(2)}) collective-permute-start(bf16[2,128,256]{2,1,0:T(8,128)(2,1)} %get-tuple-element.11), channel_id=1, source_target_pairs={{0,1},{1,2},{2,3},{3,4},{4,5},{5,6},{6,7},{7,8},{8,9},{9,10},{10,1... | collective-permute-start | bytes 393224 | tf_op jit(solution)/shard_map/ppermute | solution.py:20
  62.5 5.3 %collective-permute-start.1 = (bf16[2,128,256]{2,1,0:T(8,128)(2,1)}, bf16[2,128,256]{2,1,0:T(8,128)(2,1)}, u32[]{:S(2)}, u32[]{:S(2)}) collective-permute-start(bf16[2,128,256]{2,1,0:T(8,128)(2,1)} %get-tuple-element.12), channel_id=1, source_target_pairs={{1,0},{2,1},{3,2},{4,3},{5,4},{6,5},{7,6},{8,7},{9,8},{10,9},{11,1... | collective-permute-start | bytes 393224 | tf_op jit(solution)/shard_map/ppermute | solution.py:21
  67.9 0.6 fusion.43
  68.4 4.0 %fusion.58 = f32[288,1024]{1,0:T(8,128)S(1)} fusion(bf16[2048,1024]{1,0:T(8,128)(2,1)} %param.19, bf16[288,2048]{1,0:T(8,128)(2,1)} %param.13, f32[2048]{0:T(1024)S(1)} %bitcast.103, f32[2048]{0:T(1024)S(1)} %bitcast.106, f32[2048]{0:T(1024)S(1)} %copy-done.14, f32[288]{0:T(512)S(1)} %copy-done.19), kind=kOutput, calls=%fused_computation.114 | convolution fusion | flops 1211498496 | bytes 6579328 | tf_op jit(solution)/shard_map/dot_general | solution.py:157
  72.4 1.0 copy-done.3
  73.5 1.6 %reshape.285 = f32[288,2,4,128]{3,2,1,0:T(4,128)} reshape(f32[288,1024]{1,0:T(8,128)S(1)} %fusion.58) | data formatting | bytes 2359296 | tf_op jit(solution)/shard_map/reshape | solution.py:47
  75.0 1.7 %copy.71 = f32[288,1024]{0,1:T(8,128)S(1)} copy(f32[288,1024]{1,0:T(8,128)} %copy-done.3) | data formatting | bytes 2359296 | tf_op jit(solution)/shard_map/dot_general | solution.py:157
  76.9 2.4 %copy.90 = bf16[256,2048]{1,0:T(8,128)(2,1)} copy(bf16[256,2048]{0,1:T(8,128)(2,1)} %bitcast.96) | data formatting | bytes 2097152 | tf_op jit(solution)/shard_map/dot_general | solution.py:172
  79.5 0.3 multiply_multiply_fusion
  79.9 1.4 %copy.76 = f32[288,2,4,32]{3,0,2,1:T(8,128)} copy(f32[288,2,4,32]{0,3,2,1:T(8,128)S(1)} %bitcast.91) | data formatting | bytes 589824 | tf_op jit(solution)/shard_map/concatenate | solution.py:42
  81.3 1.4 %copy.73 = f32[288,2,4,32]{3,0,2,1:T(8,128)} copy(f32[288,2,4,32]{0,3,2,1:T(8,128)S(1)} %bitcast.90) | data formatting | bytes 589824 | tf_op jit(solution)/shard_map/concatenate | solution.py:42
  82.7 1.4 %copy.75 = f32[288,2,4,32]{3,0,2,1:T(8,128)} copy(f32[288,2,4,32]{0,3,2,1:T(8,128)S(1)} %bitcast.89) | data formatting | bytes 589824 | tf_op jit(solution)/shard_map/concatenate | solution.py:42
  84.1 1.4 %copy.74 = f32[288,2,4,32]{3,0,2,1:T(8,128)} copy(f32[288,2,4,32]{0,3,2,1:T(8,128)S(1)} %bitcast.88) | data formatting | bytes 589824 | tf_op jit(solution)/shard_map/concatenate | solution.py:42
  85.5 3.7 %fusion.13 = bf16[288,2,4,128]{3,0,2,1:T(8,128)(2,1)S(1)} fusion(f32[288,2,4,32]{3,0,2,1:T(8,128)} %copy.76, f32[288,2,4,32]{3,0,2,1:T(8,128)} %copy.75, f32[288,2,4,32]{3,0,2,1:T(8,128)} %copy.74, f32[288,2,4,32]{3,0,2,1:T(8,128)} %copy.73, f32[288,2,4,128]{3,2,1,0:T(4,128)S(1)} %copy-done.2, f32[288,128]{1,0:T(8,128)S(1)} %get-tuple-element.18, ...), kind=kLoop, calls=%fused_computation.25 | loop fusion | flops 2654208 | bytes 3253760 | tf_op jit(solution)/shard_map/convert_element_type | solution.py:161
  89.2 0.3 fusion.18
  89.5 1.0 pad_maximum_fusion
  90.8 3.8 %fusion.1 = (f32[2,4,288]{2,1,0:T(4,128)S(1)}, f32[2,544,288,4]{1,2,3,0:T(8,128)}) fusion(pred[288,544]{1,0:T(8,128)(4,1)S(1)} %fusion.18, bf16[288,2,4,128]{3,0,2,1:T(8,128)(2,1)S(1)} %fusion.13, bf16[544,2,128,1]{2,1,0,3:T(2,128)(2,1)S(1)} %bitcast.95), kind=kOutput, calls=%fused_computation.4 | convolution fusion | flops 324622080 | bytes 6047744 | tf_op jit(solution)/shard_map/rhgd,khd->hgrk/dot_general | solution.py:86
  94.6 1.5 %reshape.298 = bf16[32,1,2048]{2,1,0:T(2,128)(2,1)S(1)} reshape(bf16[32,2,1024]{2,1,0:T(2,128)(2,1)} %all-to-all-done) | data formatting | bytes 262144
  96.0 0.3 convolution_convert_fusion.1
  96.4 0.5 multiply_reduce_fusion.2
  96.9 0.4 fusion.65
  97.5 4.1 %fusion = f32[2,4,288]{2,1,0:T(4,128)S(1)} fusion(f32[2,544,288,4]{1,2,3,0:T(8,128)} %get-tuple-element.25, f32[2,4,288]{2,1,0:T(4,128)S(1)} %maximum_maximum_fusion, pred[288,544]{1,0:T(8,128)(4,1)S(1)} %fusion.18), kind=kLoop, calls=%fused_computation.3 | loop fusion | flops 5011200 | bytes 5188608 | tf_op jit(solution)/shard_map/reduce_sum | solution.py:105
  101.9 1.7 %fusion.2 = f32[2,128,4,288]{1,3,2,0:T(8,128)S(1)} fusion(f32[2,544,288,4]{1,2,3,0:T(8,128)S(1)} %copy-done.1, f32[2,4,288]{2,1,0:T(4,128)S(1)} %exponential_add_fusion, f32[2,4,288]{2,1,0:T(4,128)S(1)} %maximum_maximum_fusion, pred[288,544]{1,0:T(8,128)(4,1)S(1)} %fusion.18, bf16[544,2,128,1]{2,1,0,3:T(2,128)(2,1)S(1)} %bitcast.97), kind=kOutput, calls=%fused_computation.8 | convolution fusion | flops 327131136 | bytes 6646784 | tf_op jit(solution)/shard_map/hgrk,khd->rhgd/dot_general | solution.py:111
  103.6 0.4 fusion.10
  104.0 0.3 copy.81
  104.3 0.4 reshape.289
  104.8 0.5 copy-done.8
  105.3 4.6 %fusion.3 = bf16[288,2048]{1,0:T(8,128)(2,1)} fusion(bf16[288,1024]{1,0:T(8,128)(2,1)S(1)} %reshape.289, bf16[1024,2048]{1,0:T(8,128)(2,1)} %param.22, bf16[288,2048]{1,0:T(8,128)(2,1)S(1)} %copy-done.8, f32[2048]{0:T(1024)S(1)} %bitcast.100), kind=kOutput, calls=%fused_computation.10 | convolution fusion | flops 1210318848 | bytes 7151616 | tf_op jit(solution)/shard_map/dot_general | solution.py:195
  (70 shorter events, 2.0 us)
Async XLA Ops:
  0.0 53.4 %copy-start = (bf16[2048,256]{1,0:T(8,128)(2,1)S(1)}, bf16[2048,256]{1,0:T(8,128)(2,1)}, u32[]{:S(2)}) copy-start(bf16[2048,256]{1,0:T(8,128)(2,1)} %param.21) | copy-start | bytes 3145732
  0.0 53.1 %copy-start.16 = (f32[128]{0:T(128)S(1)}, f32[128]{0:T(128)}, u32[]{:S(2)}) copy-start(f32[128]{0:T(128)} %param.24) | copy-start | bytes 1540
  0.0 53.1 %copy-start.7 = (bf16[288,2048]{1,0:T(8,128)(2,1)S(1)}, bf16[288,2048]{1,0:T(8,128)(2,1)}, u32[]{:S(2)}) copy-start(bf16[288,2048]{1,0:T(8,128)(2,1)} %param.13) | copy-start | bytes 3538948
  2.2 51.3 %copy-start.14 = (f32[2048]{0:T(1024)S(1)}, f32[2048]{0:T(1024)}, u32[]{:S(2)}) copy-start(f32[2048]{0:T(1024)} %param.18) | copy-start | bytes 24580
  46.9 47.7 %all-to-all-start = ((bf16[32,2,1024]{2,1,0:T(2,128)(2,1)}), bf16[32,2,1024]{2,1,0:T(2,128)(2,1)}, u32[]{:S(2)}, u32[]{:S(2)}) async-start(bf16[32,2,1024]{2,1,0:T(2,128)(2,1)} %reshape.297), calls=%async_computation | async-start | bytes 262144 | tf_op jit(solution)/shard_map/all_to_all | solution.py:167
  53.4 0.7 copy-start.18
  53.5 1.2 %copy-start.11 = (bf16[2048,256]{1,0:T(8,128)(2,1)S(1)}, bf16[2048,256]{1,0:T(8,128)(2,1)}, u32[]{:S(2)}) copy-start(bf16[2048,256]{1,0:T(8,128)(2,1)} %param.20) | copy-start | bytes 3145732
  54.7 5.1 %copy-start.12 = (bf16[1,288,256]{2,1,0:T(8,128)(2,1)}, bf16[1,288,256]{2,1,0:T(8,128)(2,1)S(1)}, u32[]{:S(2)}) copy-start(bf16[1,288,256]{2,1,0:T(8,128)(2,1)S(1)} %fusion.16) | copy-start | bytes 442372
  55.3 0.7 copy-start.9
  57.5 2.1 %copy-start.10 = (f32[288,256]{1,0:T(8,128)S(1)}, f32[288,256]{1,0:T(8,128)}, u32[]{:S(2)}) copy-start(f32[288,256]{1,0:T(8,128)} %copy-done.9) | copy-start | bytes 884740
  58.2 1.6 %copy-start.5 = (f32[288,128]{1,0:T(8,128)}, f32[288,128]{1,0:T(8,128)S(1)}, u32[]{:S(2)}) copy-start(f32[288,128]{1,0:T(8,128)S(1)} %get-tuple-element.17) | copy-start | bytes 442372
  59.2 9.3 %copy-start.19 = (f32[288]{0:T(512)S(1)}, f32[288]{0:T(512)}, u32[]{:S(2)}) copy-start(f32[288]{0:T(512)} %copy-done.18) | copy-start | bytes 3460
  60.5 29.0 %collective-permute-start = (bf16[2,128,256]{2,1,0:T(8,128)(2,1)}, bf16[2,128,256]{2,1,0:T(8,128)(2,1)}, u32[]{:S(2)}, u32[]{:S(2)}) collective-permute-start(bf16[2,128,256]{2,1,0:T(8,128)(2,1)} %get-tuple-element.11), channel_id=1, source_target_pairs={{0,1},{1,2},{2,3},{3,4},{4,5},{5,6},{6,7},{7,8},{8,9},{9,10},{10,1... | collective-permute-start | bytes 393224 | tf_op jit(solution)/shard_map/ppermute | solution.py:20
  62.5 27.0 %collective-permute-start.1 = (bf16[2,128,256]{2,1,0:T(8,128)(2,1)}, bf16[2,128,256]{2,1,0:T(8,128)(2,1)}, u32[]{:S(2)}, u32[]{:S(2)}) collective-permute-start(bf16[2,128,256]{2,1,0:T(8,128)(2,1)} %get-tuple-element.12), channel_id=1, source_target_pairs={{1,0},{2,1},{3,2},{4,3},{5,4},{6,5},{7,6},{8,7},{9,8},{10,9},{11,1... | collective-permute-start | bytes 393224 | tf_op jit(solution)/shard_map/ppermute | solution.py:21
  72.4 1.0 copy-start.3
  75.0 1.8 %copy-start.21 = (f32[8]{0:T(128)S(1)}, f32[8]{0:T(128)}, u32[]{:S(2)}) copy-start(f32[8]{0:T(128)} %param.25) | copy-start | bytes 100
  76.9 2.6 %copy-start.20 = (f32[128]{0:T(128)S(1)}, f32[128]{0:T(128)}, u32[]{:S(2)}) copy-start(f32[128]{0:T(128)} %param.23) | copy-start | bytes 1540
  82.7 2.8 %copy-start.2 = (f32[288,2,4,128]{3,2,1,0:T(4,128)S(1)}, f32[288,2,4,128]{3,2,1,0:T(4,128)}, u32[]{:S(2)}) copy-start(f32[288,2,4,128]{3,2,1,0:T(4,128)} %reshape.285) | copy-start | bytes 3538948
  84.1 1.4 %copy-start.6 = (f32[288,128]{1,0:T(8,128)S(1)}, f32[288,128]{1,0:T(8,128)}, u32[]{:S(2)}) copy-start(f32[288,128]{1,0:T(8,128)} %copy-done.5) | copy-start | bytes 442372
  85.5 3.7 %copy-start.15 = (pred[544]{0:T(1024)(128)(4,1)S(1)}, pred[544]{0:T(1024)(128)(4,1)}, u32[]{:S(2)}) copy-start(pred[544]{0:T(1024)(128)(4,1)} %get-tuple-element.33) | copy-start | bytes 1636
  85.5 4.0 %copy-start.13 = (bf16[1,288,256]{2,1,0:T(8,128)(2,1)S(1)}, bf16[1,288,256]{2,1,0:T(8,128)(2,1)}, u32[]{:S(2)}) copy-start(bf16[1,288,256]{2,1,0:T(8,128)(2,1)} %copy-done.12) | copy-start | bytes 442372
  94.6 1.8 %copy-start.4 = (bf16[256,2048]{1,0:T(8,128)(2,1)S(1)}, bf16[256,2048]{1,0:T(8,128)(2,1)}, u32[]{:S(2)}) copy-start(bf16[256,2048]{1,0:T(8,128)(2,1)} %copy.90) | copy-start | bytes 3145732
  94.6 2.3 %copy-start.17 = (f32[128]{0:T(128)S(1)}, f32[128]{0:T(128)}, u32[]{:S(2)}) copy-start(f32[128]{0:T(128)} %param.24) | copy-start | bytes 1540
  97.5 4.4 %copy-start.1 = (f32[2,544,288,4]{1,2,3,0:T(8,128)S(1)}, f32[2,544,288,4]{1,2,3,0:T(8,128)}, u32[]{:S(2)}) copy-start(f32[2,544,288,4]{1,2,3,0:T(8,128)} %get-tuple-element.25) | copy-start | bytes 15040516
  104.0 1.3 %copy-start.8 = (bf16[288,2048]{1,0:T(8,128)(2,1)S(1)}, bf16[288,2048]{1,0:T(8,128)(2,1)}, u32[]{:S(2)}) copy-start(bf16[288,2048]{1,0:T(8,128)(2,1)} %param.13) | copy-start | bytes 3538948
